TPU v7x, 512 devices: a whole 4x8x8 slice. The times are simulated.
512 devices in a mesh: sp: 32 (over z, x), tp: 16 (over y, core).
Axes of the slice: x: 4, y: 8, z: 8, core: 2. Of those that a mesh axis runs over, the one named last changes fastest.
Arguments:
- queries: bfloat16 [8192, 1536], P('sp', 'tp'), may hold values from -500 to 500
- latent: bfloat16 [8192, 256], P('sp'), may hold values from -6 to 6
- rope_key: bfloat16 [8192, 32], P('sp'), may hold values from -6 to 6
- latent_gain: bfloat16 [256], replicated, may hold values from 0.099609375 to 1.8984375
- key_value_weight: bfloat16 [256, 2048], P(None, 'tp'), may hold values from -0.375 to 0.375
- out_weight: bfloat16 [1024, 2048], P(None, 'tp'), may hold values from -6 to 6
- residual: bfloat16 [8192, 2048], P('sp', 'tp'), may hold values from -150 to 150
- ffn_gain: bfloat16 [2048], replicated, may hold values from 0.099609375 to 1.8984375
- routes: int32 [8192, 2], P('sp'), may hold values from 0 to 31, all different within a row; in each aligned block of 256 rows (0 to 255, 256 to 511, ...) at most 32 rows name the same one
- route_prob: float32 [8192, 2], P('sp'), may hold values from 0.1 to 1
- group_weight: float32 [8192], P('sp'), may hold values from 0.25 to 1
- gate_weight: bfloat16 [32, 2048, 4096], P('sp', None, 'tp'), may hold values from -0.125 to 0.125
- up_weight: bfloat16 [32, 2048, 4096], P('sp', None, 'tp'), may hold values from -0.125 to 0.125
- down_weight: bfloat16 [32, 4096, 2048], P('sp', None, 'tp'), may hold values from -0.75 to 0.75
Outputs:
- final: bfloat16 [8192, 2048], P('sp', 'tp')
Inputs may be any that keep to these rules, and one draw needn't show every extreme that they name: `routes`: each row names 2 different experts; among the 256 rows of one index of sp no expert is named more than 32 times, a bound that some block reaches.
All inputs are finite; a program needn't handle non-finite values.
Results may differ from a plain program's by a relative error of at most 0.015.
The roundings to bfloat16 on the way count: a program that leaves them out, or rounds other values in their place, can miss the bound.
Values may be sent and summed in bfloat16 or wider, within the bound.
No kernel may reach another device: no remote copies, remote signals or barrier semaphores. Data moves between devices by JAX's collectives and lax.ppermute only.
A program may use at most 64 MiB of HBM per device.

v0:
```python
import jax
import jax.numpy as jnp
from jax import lax
from jax.sharding import PartitionSpec as P

D = 2048
NOPE = 64
ROPE = 32
VDIM = 64
TOP = 2
SPAN = 64
EXP_DEV = 1
THETA = 500000.0
EPSILON = 1e-06


def rotate(values, positions):
    rot_width = values.shape[-1]
    half_width = rot_width // 2
    frequency = 1.0 / THETA ** (jnp.arange(0, rot_width, 2, dtype=jnp.float32) / rot_width)
    angles = positions.astype(jnp.float32)[:, None] * frequency[None, :]
    view_shape = (values.shape[0],) + (1,) * (values.ndim - 2) + (half_width,)
    cos_table = jnp.cos(angles).reshape(view_shape)
    sin_table = jnp.sin(angles).reshape(view_shape)
    wide = values.astype(jnp.float32)
    lower_half = wide[..., :half_width]
    upper_half = wide[..., half_width:]
    return jnp.concatenate(
        [
            lower_half * cos_table - upper_half * sin_table,
            upper_half * cos_table + lower_half * sin_table,
        ],
        axis=-1,
    )


def body(
    queries,
    latent,
    rope_key,
    latent_gain,
    key_value_weight,
    out_weight,
    residual,
    ffn_gain,
    routes,
    route_prob,
    group_weight,
    gate_weight,
    up_weight,
    down_weight,
):
    tokens_here = queries.shape[0]
    heads_here = key_value_weight.shape[1] // (NOPE + VDIM)
    width_here = residual.shape[1]
    offset = lax.axis_index("sp") * tokens_here
    positions = offset + jnp.arange(tokens_here, dtype=jnp.int32)
    query = queries.reshape(tokens_here, heads_here, NOPE + ROPE)
    query_nope = query[..., :NOPE]
    query_rope = rotate(query[..., NOPE:], positions).astype(jnp.bfloat16)
    query_blocks = positions // SPAN
    last_block = query_blocks[-1]
    scaling = (NOPE + ROPE) ** (-0.5)

    def attend(state_in, key_value, rotated):
        length = rotated.shape[0]
        running_max, normalizer, weighted = state_in
        key_value = key_value.reshape(length, heads_here, NOPE + VDIM)
        scores = jnp.einsum(
            "qhd,khd->qhk", query_nope, key_value[..., :NOPE], preferred_element_type=jnp.float32
        )
        scores = scores + jnp.einsum(
            "qhd,kd->qhk", query_rope, rotated, preferred_element_type=jnp.float32
        )
        scores = scores * scaling
        key_blocks = jnp.arange(length, dtype=jnp.int32) // SPAN
        allowed = key_blocks[None, :] <= query_blocks[:, None]
        scores = jnp.where(allowed[:, None, :], scores, -jnp.inf)
        new_max = jnp.maximum(running_max, jnp.max(scores, axis=-1))
        exp_scores = jnp.exp(scores - new_max[..., None])
        normalizer = jnp.sum(exp_scores, axis=-1)
        weighted = jnp.einsum(
            "qhk,khd->qhd",
            exp_scores.astype(jnp.bfloat16),
            key_value[..., NOPE:],
            preferred_element_type=jnp.float32,
        )
        return (new_max, normalizer, weighted)

    initial = (
        jnp.full((tokens_here, heads_here), -1e30, jnp.float32),
        jnp.zeros((tokens_here, heads_here), jnp.float32),
        jnp.zeros((tokens_here, heads_here, VDIM), jnp.float32),
    )
    length = latent.shape[0]
    latent_wide = latent.astype(jnp.float32)
    normed = latent_wide * lax.rsqrt(
        jnp.mean(latent_wide * latent_wide, axis=-1, keepdims=True) + EPSILON
    )
    normed = (normed * latent_gain.astype(jnp.float32)).astype(jnp.bfloat16)
    key_value = jnp.dot(normed, key_value_weight, preferred_element_type=jnp.float32).astype(
        jnp.bfloat16
    )
    rotated = rotate(rope_key, offset + jnp.arange(length, dtype=jnp.int32)).astype(jnp.bfloat16)
    pieces = (
        lax.all_gather(key_value, "sp", axis=0, tiled=True),
        lax.all_gather(rotated, "sp", axis=0, tiled=True),
    )

    def attend_piece(kept):
        return attend(kept, pieces[0], pieces[1])

    running_max, normalizer, weighted = lax.cond(
        jnp.int32(0) // SPAN > last_block, lambda kept: kept, attend_piece, initial
    )
    attended = (
        (weighted / normalizer[..., None])
        .astype(jnp.bfloat16)
        .reshape(tokens_here, heads_here * VDIM)
    )
    projected = jnp.dot(
        lax.all_gather(attended, "tp", axis=1, tiled=True),
        out_weight,
        preferred_element_type=jnp.float32,
    )
    mixed_rows = (residual.astype(jnp.float32) + projected).astype(jnp.bfloat16)
    mixed_wide = mixed_rows.astype(jnp.float32)
    sp_count = lax.axis_size("sp")
    experts_all = EXP_DEV * sp_count
    capacity = 2 * tokens_here * TOP // experts_all
    picks = routes.reshape(-1)
    onehot = (picks[:, None] == jnp.arange(experts_all, dtype=jnp.int32)[None, :]).astype(jnp.int32)
    slot_index = jnp.sum((jnp.cumsum(onehot, axis=0) - 1) * onehot, axis=1)
    target = picks * capacity + slot_index
    token_of = jnp.arange(tokens_here * TOP, dtype=jnp.int32) // TOP
    row_shape = (sp_count, EXP_DEV, capacity)

    def place(source_rows):
        empty = jnp.zeros((experts_all * capacity,) + source_rows.shape[1:], source_rows.dtype)
        filled = empty.at[target].set(source_rows[token_of])
        return filled.reshape((sp_count, EXP_DEV * capacity) + source_rows.shape[1:])

    row_squares = lax.psum(jnp.sum(mixed_wide * mixed_wide, axis=-1), "tp")
    row_scale = lax.rsqrt(row_squares / D + EPSILON)
    gain_here = lax.dynamic_slice_in_dim(
        ffn_gain, lax.axis_index("tp") * width_here, width_here, 0
    ).astype(jnp.float32)
    scaled = (mixed_wide * gain_here[None, :]).astype(jnp.bfloat16)
    arrived_rows, arrived_scale = (
        lax.all_to_all(place(scaled), "sp", split_axis=0, concat_axis=0, tiled=True),
        lax.all_to_all(
            place(row_scale).astype(jnp.bfloat16), "sp", split_axis=0, concat_axis=0, tiled=True
        ).astype(jnp.float32),
    )
    part_rows = lax.all_gather(arrived_rows, "tp", axis=2, tiled=True)
    inputs = part_rows.reshape(row_shape + (part_rows.shape[2],))
    length = inputs.shape[3]
    gate_acc = jnp.einsum("secd,edf->secf", inputs, gate_weight, preferred_element_type=jnp.float32)
    up_acc = jnp.einsum("secd,edf->secf", inputs, up_weight, preferred_element_type=jnp.float32)
    row_scales = arrived_scale.reshape(row_shape)
    gate_full = gate_acc * row_scales[..., None]
    up_full = up_acc * row_scales[..., None]
    hidden = (jax.nn.silu(gate_full) * up_full).astype(jnp.bfloat16)
    expert_out = jnp.einsum(
        "secf,efd->secd",
        lax.all_gather(hidden, "tp", axis=3, tiled=True),
        down_weight,
        preferred_element_type=jnp.float32,
    ).astype(jnp.bfloat16)
    returned_rows = lax.all_to_all(
        expert_out.reshape(sp_count, EXP_DEV * capacity, width_here),
        "sp",
        split_axis=0,
        concat_axis=0,
        tiled=True,
    )
    picked = (
        returned_rows.reshape(experts_all * capacity, width_here)[target]
        .astype(jnp.float32)
        .reshape(tokens_here, TOP, width_here)
    )
    combine = group_weight[:, None] * route_prob / jnp.sum(route_prob, axis=-1, keepdims=True)
    routed_sum = jnp.sum(combine[..., None] * picked, axis=1)
    return (mixed_wide + routed_sum).astype(jnp.bfloat16)


def solution(mesh):
    return jax.shard_map(
        body,
        mesh=mesh,
        in_specs=(
            P("sp", "tp"),
            P("sp", None),
            P("sp", None),
            P(),
            P(None, "tp"),
            P(None, "tp"),
            P("sp", "tp"),
            P(),
            P("sp", None),
            P("sp", None),
            P("sp"),
            P("sp", None, "tp"),
            P("sp", None, "tp"),
            P("sp", None, "tp"),
        ),
        out_specs=P("sp", "tp"),
        check_vma=False,
    )
```

profile of v0, /device:TPU:8, one launch (start us, length us, event | category | flops | bytes accessed | tf_op | source)
XLA Modules:
  0.0 303.7 jit_solution(12168150198286247200)
XLA Ops:
  8.3 1.8 convolution_convert_fusion
  14.2 1.2 reduce-window.6
  18.6 50.2 %all_gather.16 = bf16[8192,32]{0,1:T(8,128)(2,1)S(1)} all-gather(bf16[256,32]{0,1:T(8,128)(2,1)S(1)} %pad_maximum_fusion.1), channel_id=1, replica_groups=mesh['sp'=32,'tp'=16] {'sp'}, dimensions={0}, use_global_device_ids=true | all-gather | bytes 540672 | tf_op jit(solution)/shard_map/all_gather | solution.py:107
  68.7 30.5 %all-gather.5.cloned.1.call-done = bf16[8192,128]{1,0:T(8,128)(2,1)} async-done(((bf16[256,128]{1,0:T(8,128)(2,1)}), bf16[8192,128]{1,0:T(8,128)(2,1)}) %all-gather.5.cloned.1.call-update) | async-done | bytes 2097168 | tf_op jit(solution)/shard_map/all_gather | solution.py:106
  99.3 6.8 %conditional.1 = (f32[256,1]{0,1:T(1,128)S(1)}, f32[256,1,64]{0,2,1:T(8,128)S(1)}) conditional(s32[]{:T(128)} %bitcast.13, (s32[256]{0:T(256)S(1)}, bf16[8192,128]{1,0:T(8,128)(2,1)}, bf16[256,1,96]{0,2,1:T(8,128)(2,1)}, bf16[256,1,32]{0,2,1:T(8,128)(2,1)S(1)}, bf16[8192,32]{0,1:T(8,128)(2,1)S(1)}) %tuple.30, () %tuple.14), branch_computations={%region_1.4_spmd, %region_4.5_spmd} | conditional | flops 690028288 | bytes 55434312 | solution.py:113
  99.3 1.3 convolution_bitcast_fusion
  100.9 1.9 fusion.67
  102.9 2.0 fusion.9
  104.9 1.2 fusion.4
  106.1 17.3 %all-gather = bf16[256,1,1024]{0,2,1:T(8,128)(2,1)S(1)} all-gather(bf16[256,1,64]{0,2,1:T(8,128)(2,1)S(1)} %divide_convert_fusion), channel_id=2, replica_groups=mesh['sp'=32,'tp'=16] {'tp'}, dimensions={2}, use_global_device_ids=true | all-gather | bytes 557056 | tf_op jit(solution)/shard_map/all_gather | solution.py:122
  123.7 3.1 %scatter_custom_fusion = bf16[1024,128]{1,0:T(8,128)(2,1)S(1)} fusion(s32[512]{0:T(512)S(1)} %bitcast.133, bf16[256,128]{1,0:T(8,128)(2,1)S(1)} %copy.51, s32[1024]{0:T(1024)S(1)} %pad_clamp_fusion.1, bf16[]{:T(256)} %constant.117.clone.1), kind=kCustom, calls=%fused_computation.56 | custom fusion | bytes 262146 | tf_op jit(solution)/shard_map/scatter | solution.py:140
  126.8 18.9 %all_to_all.16 = bf16[32,32,128]{2,1,0:T(8,128)(2,1)} all-to-all(bf16[32,32,128]{2,1,0:T(8,128)(2,1)S(1)} %bitcast.127), channel_id=1, replica_groups=mesh['sp'=32,'tp'=16] {'sp'}, dimensions={0} | all-to-all | bytes 524288 | tf_op jit(solution)/shard_map/all_to_all | solution.py:150
  145.8 22.2 %psum.7 = f32[256]{0:T(256)S(1)} all-reduce(f32[256]{0:T(256)S(1)} %get-tuple-element.37), channel_id=1, replica_groups=mesh['sp'=32,'tp'=16] {'tp'}, use_global_device_ids=true, to_apply=%region_11.12 | all-reduce | flops 256 | bytes 2048 | tf_op jit(solution)/shard_map/psum | solution.py:143
  167.9 3.5 %gather_fusion = f32[512]{0:T(512)S(1)} fusion(f32[256]{0:T(256)S(1)} %add_rsqrt_fusion, s32[1024]{0:T(1024)S(1)} %pad_clamp_fusion.1), kind=kCustom, calls=%fused_computation.1 | custom fusion | bytes 6144 | tf_op jit(solution)/shard_map/gather | solution.py:140
  171.5 2.4 scatter_custom_fusion.1
  174.0 13.8 %all_to_all.17 = bf16[32,1,32]{2,1,0:T(2,128)(2,1)S(1)} all-to-all(bf16[32,1,32]{2,1,0:T(2,128)(2,1)S(1)} %convert_element_type.138), channel_id=1, replica_groups=mesh['sp'=32,'tp'=16] {'sp'}, dimensions={0} | all-to-all | bytes 4096 | tf_op jit(solution)/shard_map/all_to_all | solution.py:151
  187.8 3.1 %all-gather.7.cloned.1.call-done = bf16[32,32,2048]{2,1,0:T(8,128)(2,1)} async-done(((bf16[32,32,128]{2,1,0:T(8,128)(2,1)}), bf16[32,32,2048]{2,1,0:T(8,128)(2,1)}) %all-gather.7.cloned.1.call-update) | async-done | bytes 4194320 | tf_op jit(solution)/shard_map/all_gather | solution.py:155
  190.9 3.5 %fusion.23 = f32[32,1,32,256]{3,2,0,1:T(8,128)S(1)} fusion(bf16[32,32,2048]{2,1,0:T(8,128)(2,1)} %all-gather.7.cloned.1.call-done, bf16[1,2048,256]{2,1,0:T(8,128)(2,1)S(1)} %copy-done, f32[32,32]{1,0:T(8,128)S(1)} %bitcast.131), kind=kOutput, calls=%fused_computation.37 | convolution fusion | flops 1074003968 | bytes 6295552 | tf_op jit(solution)/shard_map/secd,edf->secf/dot_general | solution.py:158
  194.4 4.4 %fusion.25 = bf16[32,1,32,256]{3,2,0,1:T(8,128)(2,1)} fusion(bf16[32,32,2048]{2,1,0:T(8,128)(2,1)} %all-gather.7.cloned.1.call-done, bf16[1,2048,256]{2,1,0:T(8,128)(2,1)S(1)} %copy-done.6, f32[32,1,32,256]{3,2,0,1:T(8,128)S(1)} %fusion.23, f32[32,32]{1,0:T(8,128)S(1)} %bitcast.132), kind=kOutput, calls=%fused_computation.39 | convolution fusion | flops 1075576832 | bytes 6819840 | tf_op jit(solution)/shard_map/secd,edf->secf/dot_general | solution.py:159
  198.8 66.5 %all-gather.9.cloned.1.call-done = bf16[32,1,32,4096]{3,2,0,1:T(8,128)(2,1)} async-done(((bf16[32,1,32,256]{3,2,0,1:T(8,128)(2,1)}), bf16[32,1,32,4096]{3,2,0,1:T(8,128)(2,1)}) %all-gather.9.cloned.1.call-update) | async-done | bytes 8388624 | tf_op jit(solution)/shard_map/all_gather | solution.py:166
  265.3 6.4 %fusion.26 = bf16[32,32,128]{2,1,0:T(8,128)(2,1)} fusion(bf16[32,1,32,4096]{3,2,0,1:T(8,128)(2,1)} %all-gather.9.cloned.1.call-done, bf16[1,4096,128]{2,1,0:T(8,128)(2,1)S(1)} %copy-done.7), kind=kOutput, calls=%fused_computation.40 | convolution fusion | flops 1073872896 | bytes 9699328 | tf_op jit(solution)/shard_map/secf,efd->secd/dot_general | solution.py:164
  271.8 9.4 %all-to-all-start.2 = ((bf16[32,32,128]{2,1,0:T(8,128)(2,1)}), bf16[32,32,128]{2,1,0:T(8,128)(2,1)S(1)}, u32[]{:S(2)}, u32[]{:S(2)}) async-start(bf16[32,32,128]{2,1,0:T(8,128)(2,1)} %fusion.26), calls=%async_computation.2 | async-start | bytes 524288 | tf_op jit(solution)/shard_map/all_to_all | solution.py:170
  281.4 13.2 %all-to-all-done.2 = bf16[32,32,128]{2,1,0:T(8,128)(2,1)S(1)} async-done(((bf16[32,32,128]{2,1,0:T(8,128)(2,1)}), bf16[32,32,128]{2,1,0:T(8,128)(2,1)S(1)}, u32[]{:S(2)}, u32[]{:S(2)}) %all-to-all-start.2) | async-done | bytes 262176 | tf_op jit(solution)/shard_map/all_to_all | solution.py:170
  294.6 1.3 gather_fusion.1
  (68 shorter events, 10.7 us)
Async XLA Ops:
  6.5 184.4 %copy-start = (bf16[1,2048,256]{2,1,0:T(8,128)(2,1)S(1)}, bf16[1,2048,256]{2,1,0:T(8,128)(2,1)}, u32[]{:S(2)}) copy-start(bf16[1,2048,256]{2,1,0:T(8,128)(2,1)} %param.27) | copy-start | bytes 3145732
  6.5 92.7 %all-gather.5.cloned.1.call-start = ((), (), s32[]{:S(2)}) async-start(), calls=%async_computation.3 | async-start | bytes 2162688 | tf_op jit(solution)/shard_map/all_gather | solution.py:106
  10.1 180.8 %all-gather.7.cloned.1.call-start = ((), (), s32[]{:S(2)}) async-start(), calls=%async_computation.4 | async-start | bytes 4456448 | tf_op jit(solution)/shard_map/all_gather | solution.py:155
  99.3 24.1 %copy-start.2 = (bf16[1024,128]{1,0:T(8,128)(2,1)S(1)}, bf16[1024,128]{1,0:T(8,128)(2,1)}, u32[]{:S(2)}) copy-start(bf16[1024,128]{1,0:T(8,128)(2,1)} %param.21) | copy-start | bytes 786436
  99.3 1.6 copy-start.1
  99.3 1.6 copy-start.3
  106.0 88.4 %copy-start.6 = (bf16[1,2048,256]{2,1,0:T(8,128)(2,1)S(1)}, bf16[1,2048,256]{2,1,0:T(8,128)(2,1)}, u32[]{:S(2)}) copy-start(bf16[1,2048,256]{2,1,0:T(8,128)(2,1)} %param.28) | copy-start | bytes 3145732
  145.7 119.6 %all-gather.9.cloned.1.call-start = ((), (), s32[]{:S(2)}) async-start(), calls=%async_computation.5 | async-start | bytes 8912896 | tf_op jit(solution)/shard_map/all_gather | solution.py:166
  190.9 74.5 %copy-start.7 = (bf16[1,4096,128]{2,1,0:T(8,128)(2,1)S(1)}, bf16[1,4096,128]{2,1,0:T(8,128)(2,1)}, u32[]{:S(2)}) copy-start(bf16[1,4096,128]{2,1,0:T(8,128)(2,1)} %param.29) | copy-start | bytes 3145732
  198.8 82.4 %copy-start.4 = (f32[256,2]{0,1:T(2,128)S(1)}, f32[256,2]{0,1:T(2,128)}, u32[]{:S(2)}) copy-start(f32[256,2]{0,1:T(2,128)} %param.25) | copy-start | bytes 6148
  198.8 82.4 %copy-start.5 = (f32[256]{0:T(256)S(1)}, f32[256]{0:T(256)}, u32[]{:S(2)}) copy-start(f32[256]{0:T(256)} %param.26) | copy-start | bytes 3076
  271.8 22.8 %all-to-all-start.2 = ((bf16[32,32,128]{2,1,0:T(8,128)(2,1)}), bf16[32,32,128]{2,1,0:T(8,128)(2,1)S(1)}, u32[]{:S(2)}, u32[]{:S(2)}) async-start(bf16[32,32,128]{2,1,0:T(8,128)(2,1)} %fusion.26), calls=%async_computation.2 | async-start | bytes 524288 | tf_op jit(solution)/shard_map/all_to_all | solution.py:170
Sparse Core Ops, SparseCore 0:
  10.5 88.7 all-gather.4
  145.8 45.0 all-gather.6
  199.0 66.3 all-gather.8
where the time goes:
time: 304 us
  blocking collectives  122 us (40%)
  waiting for transfers between devices  113 us (37%)
  matrix products  21.6 us (7%)
  local copies, waits for them, and re-layouts  15 us (5%)
  between operations  14 us (5%)
  starting transfers between devices  9.5 us (3%)
  other arithmetic  8.01 us (3%)
    all_gather x1, waiting for transfers between devices, body(): lax.all_gather(hidden, 'tp', axis=3, tiled=True)  66.5 us
    all_gather x1, blocking collectives, body(): lax.all_gather(rotated, 'sp', axis=0, tiled=True)  50.2 us
    all_gather x1, waiting for transfers between devices, body(): lax.all_gather(key_value, 'sp', axis=0, tiled=True)  30.5 us
    psum x1, blocking collectives, body(): row_squares = lax.psum(jnp.sum(mixed_wide * mixed_wide, axis=-1), 'tp')  22.2 us
    all_to_all x1, blocking collectives, body(): lax.all_to_all(place(scaled), 'sp', split_axis=0, concat_axis=0, tiled=True)  18.9 us
    all_gather x1, blocking collectives, body(): lax.all_gather(attended, 'tp', axis=1, tiled=True)  17.3 us
    all_to_all x1, blocking collectives, body(): lax.all_to_all(place(row_scale).astype(jnp.bfloat16), 'sp', split_axis=0,...  13.8 us
    all_to_all x1, waiting for transfers between devices, body(): lax.all_to_all(expert_out.reshape(sp_count, EXP_DEV * capacity, width_her...  13.2 us
  transfers between devices with their start and end apart: 4, of which 4 were waited for; matrix products, arithmetic and copies ran while one was open for 5% of the time, Pallas kernels for 0%

commit v1 on v0

--- a/solution.py
+++ b/solution.py
@@ -12,6 +12,14 @@
 EXP_DEV = 1
 THETA = 500000.0
 EPSILON = 1e-06
+
+
+def run_the_sums_all(here_x, at_axis):
+    arr_next = jnp.concatenate(
+        lax.all_to_all(jnp.stack([here_x for _ in range(lax.axis_size("tp"))], axis=0), "tp", 0, 0),
+        axis=at_axis,
+    )
+    return arr_next
 
 
 def rotate(values, positions):
@@ -163,7 +171,7 @@
     hidden = (jax.nn.silu(gate_full) * up_full).astype(jnp.bfloat16)
     expert_out = jnp.einsum(
         "secf,efd->secd",
-        lax.all_gather(hidden, "tp", axis=3, tiled=True),
+        run_the_sums_all(hidden, 3),
         down_weight,
         preferred_element_type=jnp.float32,
     ).astype(jnp.bfloat16)

time: 304 us -> 460 us (1.51)
  the two profiles are of different devices: /device:TPU:8 before, /device:TPU:1 now
where the time goes in v1:
time: 460 us; the launch traced here: 458 us
  blocking collectives  312 us (68%)
  waiting for transfers between devices  49 us (11%)
  local copies, waits for them, and re-layouts  44.7 us (10%)
  matrix products  20.7 us (4%)
  between operations  14.3 us (3%)
  starting transfers between devices  9.84 us (2%)
  other arithmetic  8 us (2%)
    all_to_all x1, blocking collectives, run_the_sums_all(): lax.all_to_all(jnp.stack([here_x for _ in range(lax.axis_size('tp'))], ax...  189 us
    all_gather x1, blocking collectives, body(): lax.all_gather(rotated, 'sp', axis=0, tiled=True)  43.7 us
    all_gather x1, waiting for transfers between devices, body(): lax.all_gather(key_value, 'sp', axis=0, tiled=True)  33 us
    psum x1, blocking collectives, body(): row_squares = lax.psum(jnp.sum(mixed_wide * mixed_wide, axis=-1), 'tp')  25.5 us
    all_gather x1, blocking collectives, body(): lax.all_gather(attended, 'tp', axis=1, tiled=True)  24 us
    all_to_all x1, blocking collectives, body(): lax.all_to_all(place(scaled), 'sp', split_axis=0, concat_axis=0, tiled=True)  16.7 us
    reshape x1, local copies, waits for them, and re-layouts, run_the_sums_all(): jnp.concatenate(lax.all_to_all(jnp.stack([here_x for _ in range(lax.axis_...  15.1 us
    another operation x2, local copies, waits for them, and re-layouts  13.6 us
  transfers between devices with their start and end apart: 3, of which 3 were waited for; matrix products, arithmetic and copies ran while one was open for 3% of the time, Pallas kernels for 0%

profile of v1, /device:TPU:1, one launch (start us, length us, event | category | flops | bytes accessed | tf_op | source)
XLA Modules:
  0.0 458.4 jit_solution(314667414025123197)
XLA Ops:
  8.3 1.8 convolution_convert_fusion.1
  18.5 43.7 %all_gather.13 = bf16[8192,32]{0,1:T(8,128)(2,1)S(1)} all-gather(bf16[256,32]{0,1:T(8,128)(2,1)S(1)} %pad_maximum_fusion.1), channel_id=1, replica_groups=mesh['sp'=32,'tp'=16] {'sp'}, dimensions={0}, use_global_device_ids=true | all-gather | bytes 540672 | tf_op jit(solution)/shard_map/all_gather | solution.py:115
  62.2 33.0 %all-gather.4.cloned.1.call-done = bf16[8192,128]{1,0:T(8,128)(2,1)} async-done(((bf16[256,128]{1,0:T(8,128)(2,1)}), bf16[8192,128]{1,0:T(8,128)(2,1)}) %all-gather.4.cloned.1.call-update) | async-done | bytes 2097168 | tf_op jit(solution)/shard_map/all_gather | solution.py:114
  95.2 6.8 %conditional.1 = (f32[256,1]{0,1:T(1,128)S(1)}, f32[256,1,64]{0,2,1:T(8,128)S(1)}) conditional(s32[]{:T(128)} %bitcast.13, (s32[256]{0:T(256)S(1)}, bf16[8192,128]{1,0:T(8,128)(2,1)}, bf16[256,1,96]{0,2,1:T(8,128)(2,1)}, bf16[256,1,32]{0,2,1:T(8,128)(2,1)S(1)}, bf16[8192,32]{0,1:T(8,128)(2,1)S(1)}) %tuple.28, () %tuple.14), branch_computations={%region_1.4_spmd, %region_4.5_spmd} | conditional | flops 690028288 | bytes 55434312 | solution.py:121
  95.2 1.3 convolution_bitcast_fusion
  96.9 2.0 fusion.63
  100.0 2.0 fusion.9
  102.0 24.0 %all-gather = bf16[256,1,1024]{0,2,1:T(8,128)(2,1)S(1)} all-gather(bf16[256,1,64]{0,2,1:T(8,128)(2,1)S(1)} %divide_convert_fusion), channel_id=2, replica_groups=mesh['sp'=32,'tp'=16] {'tp'}, dimensions={2}, use_global_device_ids=true | all-gather | bytes 557056 | tf_op jit(solution)/shard_map/all_gather | solution.py:130
  126.4 3.1 scatter_custom_fusion
  129.5 16.7 %all_to_all.21 = bf16[32,32,128]{2,1,0:T(8,128)(2,1)} all-to-all(bf16[32,32,128]{2,1,0:T(8,128)(2,1)S(1)} %bitcast.135), channel_id=1, replica_groups=mesh['sp'=32,'tp'=16] {'sp'}, dimensions={0} | all-to-all | bytes 524288 | tf_op jit(solution)/shard_map/all_to_all | solution.py:158
  146.2 25.5 %psum.7 = f32[256]{0:T(256)S(1)} all-reduce(f32[256]{0:T(256)S(1)} %get-tuple-element.37), channel_id=1, replica_groups=mesh['sp'=32,'tp'=16] {'tp'}, use_global_device_ids=true, to_apply=%region_11.12 | all-reduce | flops 256 | bytes 2048 | tf_op jit(solution)/shard_map/psum | solution.py:151
  171.7 3.5 gather_fusion
  175.2 2.4 scatter_custom_fusion.1
  177.8 12.5 %all_to_all.22 = bf16[32,1,32]{2,1,0:T(2,128)(2,1)S(1)} all-to-all(bf16[32,1,32]{2,1,0:T(2,128)(2,1)S(1)} %convert_element_type.141), channel_id=1, replica_groups=mesh['sp'=32,'tp'=16] {'sp'}, dimensions={0} | all-to-all | bytes 4096 | tf_op jit(solution)/shard_map/all_to_all | solution.py:159
  190.3 3.4 all-gather.6.cloned.1.call-done
  193.8 3.4 fusion.21
  197.2 3.5 fusion.24
  201.8 189.5 %all_to_all.23 = bf16[16,32,1,32,256]{4,3,1,2,0:T(8,128)(2,1)} all-to-all(bf16[16,32,1,32,256]{4,3,1,2,0:T(8,128)(2,1)S(1)} %stack.2), channel_id=1, replica_groups=mesh['sp'=32,'tp'=16] {'tp'}, dimensions={0} | all-to-all | bytes 16777216 | tf_op jit(solution)/shard_map/all_to_all | solution.py:19
  391.3 15.1 %copy.54 = bf16[32,1,32,16,256]{4,3,2,0,1:T(8,128)(2,1)} copy(bf16[32,1,32,16,256]{4,2,0,1,3:T(8,128)(2,1)} %bitcast.131) | data formatting | bytes 16777216 | tf_op jit(solution)/shard_map/reshape | solution.py:18
  406.4 13.6 %reshape.392 = bf16[32,32,4096]{2,1,0:T(8,128)(2,1)} reshape(bf16[32,1,32,16,256]{4,3,2,0,1:T(8,128)(2,1)} %copy.54) | data formatting | bytes 16777216 | tf_op jit(solution)/shard_map/reshape.37
  420.0 6.4 %convolution_convert_fusion = bf16[32,32,128]{2,1,0:T(8,128)(2,1)} fusion(bf16[32,32,4096]{2,1,0:T(8,128)(2,1)} %reshape.392, bf16[1,4096,128]{2,1,0:T(8,128)(2,1)S(1)} %copy-done.7), kind=kOutput, calls=%fused_computation.39 | convolution fusion | flops 1073872896 | bytes 9699328 | tf_op jit(solution)/shard_map/secf,efd->secd/dot_general | solution.py:172
  426.4 9.8 %all-to-all-start.3 = ((bf16[32,32,128]{2,1,0:T(8,128)(2,1)}), bf16[32,32,128]{2,1,0:T(8,128)(2,1)S(1)}, u32[]{:S(2)}, u32[]{:S(2)}) async-start(bf16[32,32,128]{2,1,0:T(8,128)(2,1)} %convolution_convert_fusion), calls=%async_computation.3 | async-start | bytes 524288 | tf_op jit(solution)/shard_map/all_to_all | solution.py:178
  436.4 12.5 %all-to-all-done.3 = bf16[32,32,128]{2,1,0:T(8,128)(2,1)S(1)} async-done(((bf16[32,32,128]{2,1,0:T(8,128)(2,1)}), bf16[32,32,128]{2,1,0:T(8,128)(2,1)S(1)}, u32[]{:S(2)}, u32[]{:S(2)}) %all-to-all-start.3) | async-done | bytes 262176 | tf_op jit(solution)/shard_map/all_to_all | solution.py:178
  449.0 1.3 gather_fusion.1
  (69 shorter events, 14.1 us)
Async XLA Ops:
  6.5 187.2 %copy-start = (bf16[1,2048,256]{2,1,0:T(8,128)(2,1)S(1)}, bf16[1,2048,256]{2,1,0:T(8,128)(2,1)}, u32[]{:S(2)}) copy-start(bf16[1,2048,256]{2,1,0:T(8,128)(2,1)} %param.27) | copy-start | bytes 3145732
  6.5 88.7 %all-gather.4.cloned.1.call-start = ((), (), s32[]{:S(2)}) async-start(), calls=%async_computation.4 | async-start | bytes 2162688 | tf_op jit(solution)/shard_map/all_gather | solution.py:114
  10.1 183.7 %all-gather.6.cloned.1.call-start = ((), (), s32[]{:S(2)}) async-start(), calls=%async_computation.5 | async-start | bytes 4456448 | tf_op jit(solution)/shard_map/all_gather | solution.py:163
  95.2 30.8 %copy-start.2 = (bf16[1024,128]{1,0:T(8,128)(2,1)S(1)}, bf16[1024,128]{1,0:T(8,128)(2,1)}, u32[]{:S(2)}) copy-start(bf16[1024,128]{1,0:T(8,128)(2,1)} %param.21) | copy-start | bytes 786436
  95.2 1.6 copy-start.1
  95.2 1.6 copy-start.3
  102.0 95.2 %copy-start.6 = (bf16[1,2048,256]{2,1,0:T(8,128)(2,1)S(1)}, bf16[1,2048,256]{2,1,0:T(8,128)(2,1)}, u32[]{:S(2)}) copy-start(bf16[1,2048,256]{2,1,0:T(8,128)(2,1)} %param.28) | copy-start | bytes 3145732
  406.4 13.6 %copy-start.7 = (bf16[1,4096,128]{2,1,0:T(8,128)(2,1)S(1)}, bf16[1,4096,128]{2,1,0:T(8,128)(2,1)}, u32[]{:S(2)}) copy-start(bf16[1,4096,128]{2,1,0:T(8,128)(2,1)} %param.29) | copy-start | bytes 3145732
  420.0 16.2 %copy-start.4 = (f32[256,2]{0,1:T(2,128)S(1)}, f32[256,2]{0,1:T(2,128)}, u32[]{:S(2)}) copy-start(f32[256,2]{0,1:T(2,128)} %param.25) | copy-start | bytes 6148
  420.0 16.3 %copy-start.5 = (f32[256]{0:T(256)S(1)}, f32[256]{0:T(256)}, u32[]{:S(2)}) copy-start(f32[256]{0:T(256)} %param.26) | copy-start | bytes 3076
  426.4 22.5 %all-to-all-start.3 = ((bf16[32,32,128]{2,1,0:T(8,128)(2,1)}), bf16[32,32,128]{2,1,0:T(8,128)(2,1)S(1)}, u32[]{:S(2)}, u32[]{:S(2)}) async-start(bf16[32,32,128]{2,1,0:T(8,128)(2,1)} %convolution_convert_fusion), calls=%async_computation.3 | async-start | bytes 524288 | tf_op jit(solution)/shard_map/all_to_all | solution.py:178
Sparse Core Ops, SparseCore 0:
  10.5 84.6 all-gather.3
  146.3 47.3 all-gather.5
